TPU v7x, 32 devices: a whole 2x2x4 slice. The times are simulated.
32 devices in a mesh: fs: 4 (over z), rep: 2 (over y), tp: 4 (over x, core).
Axes of the slice: x: 2, y: 2, z: 4, core: 2. Of those that a mesh axis runs over, the one named last changes fastest.
Arguments:
- saved_hidden: bfloat16 [7168, 2048], P(('fs', 'rep')), may hold values from -12 to 12
- grad_value: bfloat16 [7168, 1024], P(('fs', 'rep'), 'tp'), may hold values from -12 to 12
- saved_mixed: bfloat16 [7168, 1024], P(('fs', 'rep'), 'tp'), may hold values from -12 to 12
- grad_output: bfloat16 [7168, 2048], P(('fs', 'rep')), may hold values from -12 to 12
- basis_value: bfloat16 [2048, 128], replicated, may hold values from -0.5 to 0.5
- basis_output: bfloat16 [2048, 128], replicated, may hold values from -0.5 to 0.5
- weight_value: float32 [2048, 1024], P('fs', 'tp'), may hold values from -0.125 to 0.125
- weight_output: float32 [1024, 2048], P('tp', 'fs'), may hold values from -0.1875 to 0.1875
- first_value: float32 [128, 1024], P('fs', 'tp'), may hold values from -4 to 4
- second_value: float32 [128, 1024], P('fs', 'tp'), may hold values from 0.05 to 0.5
- first_output: float32 [128, 1024], P('fs', 'tp'), may hold values from -4 to 4
- second_output: float32 [128, 1024], P('fs', 'tp'), may hold values from 0.05 to 0.5
Outputs:
- step_value: float32 [2048, 1024], P('fs', 'tp')
- step_output: float32 [1024, 2048], P('tp', 'fs')
- new_weight_value: float32 [2048, 1024], P('fs', 'tp')
- new_weight_output: float32 [1024, 2048], P('tp', 'fs')
- copy_value: bfloat16 [2048, 1024], P(None, 'tp')
- copy_output: bfloat16 [1024, 2048], P('tp')
- new_first_value: float32 [128, 1024], P('fs', 'tp')
- new_second_value: float32 [128, 1024], P('fs', 'tp')
- new_first_output: float32 [128, 1024], P('fs', 'tp')
- new_second_output: float32 [128, 1024], P('fs', 'tp')
All inputs are finite; a program needn't handle non-finite values.
Results may differ from a plain program's by a relative error of at most 0.0045.
Values may be sent and summed in bfloat16 or wider, within the bound.
A program may use at most 64 MiB of HBM per device.

v0:
```python
import functools
import jax
import jax.numpy as jnp
from jax import lax
from jax.experimental import pallas as pl
from jax.experimental.pallas import tpu as pltpu
from jax.sharding import PartitionSpec as P

AW = 1024
RANK = 128


first_decay = 0.8
second_decay = 0.9
learning_rate = 0.02
norm_epsilon = 1e-06
contract_leading = (((0,), (0,)), ((), ()))


def moments(projected, first_old, second_old, clip_factor):
    scaled = clip_factor * projected
    first_new = first_decay * first_old + (1.0 - first_decay) * scaled
    second_new = second_decay * second_old + (1.0 - second_decay) * scaled * scaled
    return (first_new, second_new, first_new / jnp.sqrt(second_new))


def split_product(reduced, other):
    upper = reduced.astype(jnp.bfloat16)
    lower = (reduced - upper.astype(jnp.float32)).astype(jnp.bfloat16)
    rank_count = reduced.shape[1]
    stacked = jnp.concatenate([upper, lower], axis=1)
    both = lax.dot_general(stacked, other, contract_leading, preferred_element_type=jnp.float32)
    return both[:rank_count] + both[rank_count:]


def local(
    saved_hidden,
    grad_value,
    saved_mixed,
    grad_output,
    basis_value,
    basis_output,
    weight_value,
    weight_output,
    first_value,
    second_value,
    first_output,
    second_output,
):
    row_count = weight_value.shape[0]
    moment_count = first_value.shape[0]
    fs_index = lax.axis_index("fs")
    row_first = fs_index * row_count
    moment_first = fs_index * moment_count
    value_basis_rows = lax.dynamic_slice_in_dim(basis_value, row_first, row_count, 0).astype(
        jnp.float32
    )
    output_basis_rows = lax.dynamic_slice_in_dim(basis_output, row_first, row_count, 0).astype(
        jnp.float32
    )
    reduced_hidden = jnp.dot(saved_hidden, basis_value, preferred_element_type=jnp.float32)
    reduced_output = jnp.dot(grad_output, basis_output, preferred_element_type=jnp.float32)
    part_value = split_product(reduced_hidden, grad_value)
    part_output = split_product(reduced_output, saved_mixed)
    projected_value, projected_output = lax.psum((part_value, part_output), ("fs", "rep"))
    local_squares = jnp.sum(projected_value * projected_value) + jnp.sum(
        projected_output * projected_output
    )
    total_squares = lax.psum(local_squares, "tp")
    mean_square = total_squares / (2 * RANK * AW)
    clip_factor = jnp.minimum(1.0, 1.0 / jnp.sqrt(mean_square + norm_epsilon))
    value_slice = lax.dynamic_slice_in_dim(projected_value, moment_first, moment_count, 0)
    output_slice = lax.dynamic_slice_in_dim(projected_output, moment_first, moment_count, 0)
    new_first_value, new_second_value, value_direction_rows = moments(
        value_slice, first_value, second_value, clip_factor
    )
    new_first_output, new_second_output, output_direction_rows = moments(
        output_slice, first_output, second_output, clip_factor
    )
    direction_value, direction_output = (
        lax.all_gather(value_direction_rows, "fs", axis=0, tiled=True),
        lax.all_gather(output_direction_rows, "fs", axis=0, tiled=True),
    )
    step_value = jnp.dot(value_basis_rows, direction_value, precision=lax.Precision.HIGHEST)
    step_output = jnp.dot(output_basis_rows, direction_output, precision=lax.Precision.HIGHEST).T
    new_weight_value = weight_value - learning_rate * step_value
    new_weight_output = weight_output - learning_rate * step_output
    copy_value, copy_output = (
        lax.all_gather(new_weight_value.astype(jnp.bfloat16), "fs", axis=0, tiled=True),
        lax.all_gather(new_weight_output.astype(jnp.bfloat16), "fs", axis=1, tiled=True),
    )
    return (
        step_value,
        step_output,
        new_weight_value,
        new_weight_output,
        copy_value,
        copy_output,
        new_first_value,
        new_second_value,
        new_first_output,
        new_second_output,
    )


MESH = pl.DeviceIdType.MESH


def remote(src, dst, send, recv, **where):
    return pltpu.make_async_remote_copy(
        src_ref=src, dst_ref=dst, send_sem=send, recv_sem=recv, device_id=where, device_id_type=MESH
    )


def exchange(
    fs_count, rep_count, tp_count,
    hidden, grad_value, mixed, grad_output, basis_value, basis_output, weight_value, weight_output,
    first_value, second_value, first_output, second_output,
    direction, owned, clip, all_value, all_output,
    tokens_in, thin_in, basis_in, value_in, output_in, moment_in,
    part, landed, squares_all,
    load_sem, near_send, near_recv, side_send, side_recv, part_send, part_recv,
    square_send, square_recv, owned_send, owned_recv, turn_send, turn_recv,
):
    group = fs_count * rep_count
    fs, rep, tp = lax.axis_index("fs"), lax.axis_index("rep"), lax.axis_index("tp")
    me = fs * rep_count + rep
    tokens = hidden.shape[0]
    rows = part.shape[2]
    width = part.shape[3]
    half = tokens // 2

    loads = []

    def load(source, target):
        copy = pltpu.make_async_copy(source, target, load_sem.at[len(loads)])
        copy.start()
        loads.append(copy)
        return copy

    weight_loads = [load(weight_value, value_in), load(weight_output, output_in)]
    stream_loads = []
    for a, (big, thin, basis) in enumerate(
        ((hidden, grad_value, basis_value), (grad_output, mixed, basis_output))
    ):
        first = load(basis, basis_in.at[a])
        second = load(thin, thin_in.at[a])
        blocks = [
            load(big.at[pl.ds(c * half, half)], tokens_in.at[a, pl.ds(c * half, half)])
            for c in range(2)
        ]
        stream_loads.append((first, second, blocks))
    moment_loads = [
        load(source.at[pl.ds(pl.multiple_of(rep * rows, rows), rows)], moment_in.at[i])
        for i, source in enumerate((first_value, first_output, second_value, second_output))
    ]

    def member(k):
        other = lax.rem(me + k, group)
        return {"fs": other // rep_count, "rep": lax.rem(other, rep_count)}

    barrier = pltpu.get_barrier_semaphore()
    everyone = group * tp_count

    def anyone(k):
        other = lax.rem(me * tp_count + tp + k, everyone)
        place = other // tp_count
        return {
            "fs": place // rep_count, "rep": lax.rem(place, rep_count), "tp": lax.rem(other, tp_count)
        }

    for k in range(1, everyone):
        pl.semaphore_signal(barrier, inc=1, device_id=anyone(k), device_id_type=MESH)
    for copy in weight_loads:
        copy.wait()
    all_value[fs] = value_in[...].astype(jnp.bfloat16)
    all_output[fs] = output_in[...].astype(jnp.bfloat16)
    pl.semaphore_wait(barrier, everyone - 1)

    share_value = value_in.shape[0] // rep_count
    share_output = output_in.shape[0] // rep_count
    shares = (
        (all_value, pl.ds(pl.multiple_of(rep * share_value, share_value), share_value)),
        (all_output, pl.ds(pl.multiple_of(rep * share_output, share_output), share_output)),
    )
    sent = []

    def send(copy):
        copy.start()
        sent.append(copy)
        return copy

    def hop(a, way, d):
        buffer, rows_here = shares[a]
        step = 1 if way == 0 else -1
        block = buffer.at[fs - step * d, rows_here]
        return remote(
            block, block, near_send.at[a, way, d], near_recv.at[a, way, d], fs=fs + step
        )

    def arrival(a, way, d):
        buffer, rows_here = shares[a]
        step = 1 if way == 0 else -1
        block = buffer.at[fs - step * d, rows_here]
        return remote(
            block, block, near_send.at[a, way, d - 1], near_recv.at[a, way, d - 1], fs=fs - step
        )

    def across(a, way, d, j):
        buffer, rows_here = shares[a]
        step = 1 if way == 0 else -1
        block = buffer.at[fs - step * d, rows_here]
        return remote(
            block, block, side_send.at[a, way, d - 1, j - 1], side_recv.at[a, way, d - 1, j - 1],
            rep=lax.rem(rep + j, rep_count),
        )

    def reaches(way, d):
        return fs >= d if way == 0 else fs + d < fs_count

    def leaves(way, d):
        onward = fs < fs_count - 1 if way == 0 else fs > 0
        return jnp.logical_and(onward, reaches(way, d))

    def send_weights(d):
        for way in range(2):
            @pl.when(leaves(way, d))
            def _():
                for a in range(2):
                    hop(a, way, d).start()

    def pass_weights(d):
        for a in range(2):
            for way in range(2):
                @pl.when(reaches(way, d))
                def _():
                    arrival(a, way, d).wait_recv()

                if d < fs_count - 1:
                    @pl.when(leaves(way, d))
                    def _():
                        hop(a, way, d).start()

                @pl.when(reaches(way, d))
                def _():
                    for j in range(1, rep_count):
                        across(a, way, d, j).start()

    def settle_weights():
        for d in range(fs_count):
            for way in range(2):
                if d < fs_count - 1:
                    @pl.when(leaves(way, d))
                    def _():
                        for a in range(2):
                            hop(a, way, d).wait_send()

                if d > 0:
                    @pl.when(reaches(way, d))
                    def _():
                        for a in range(2):
                            for j in range(1, rep_count):
                                across(a, way, d, j).wait()

    send_weights(0)

    parts = []
    for a in range(2):
        first, second, blocks = stream_loads[a]
        first.wait()
        second.wait()
        total = None
        for c in range(2):
            blocks[c].wait()
            reduced = jnp.dot(
                tokens_in[a, pl.ds(c * half, half)], basis_in[a], preferred_element_type=jnp.float32
            )
            product = split_product(reduced, thin_in[a, pl.ds(c * half, half)])
            total = product if total is None else total + product
        part[a] = total.reshape(group, rows, width)
        for k in range(1, group):
            other = lax.rem(me + k, group)
            parts.append(send(remote(
                part.at[a, other], landed.at[a, k - 1],
                part_send.at[a, k - 1], part_recv.at[a, k - 1], **member(k),
            )))

    for d in range(1, 2):
        pass_weights(d)
    for copy in parts:
        copy.wait_recv()
    squares = jnp.zeros((rows, width), jnp.float32)
    for a in range(2):
        summed = part[a, me]
        for k in range(group - 1):
            summed = summed + landed[a, k]
        owned[rep, a] = summed
        squares = squares + summed * summed
    place = me * tp_count + tp
    squares_all[place] = jnp.full(squares_all.shape[1:], jnp.sum(squares), jnp.float32)
    square_copies = [
        send(remote(
            squares_all.at[place], squares_all.at[place],
            square_send.at[k - 1], square_recv.at[k - 1], **anyone(k),
        ))
        for k in range(1, everyone)
    ]
    owned_copies = [
        send(remote(
            owned.at[rep], owned.at[rep], owned_send.at[j - 1], owned_recv.at[j - 1],
            rep=lax.rem(rep + j, rep_count),
        ))
        for j in range(1, rep_count)
    ]
    for d in range(2, 3):
        pass_weights(d)
    for copy in moment_loads:
        copy.wait()
    for copy in square_copies:
        copy.wait_recv()
    mean_square = jnp.sum(squares_all[...], axis=0) / (2 * RANK * AW)
    factor = jnp.minimum(1.0, 1.0 / jnp.sqrt(mean_square + norm_epsilon))
    clip[...] = jnp.broadcast_to(factor, clip.shape)
    scale = factor[:1, :1]
    for a in range(2):
        _, _, turned = moments(owned[rep, a], moment_in[a], moment_in[2 + a], scale)
        direction[me, a] = turned.astype(jnp.bfloat16)
    turn_copies = [
        send(remote(
            direction.at[me], direction.at[me], turn_send.at[k - 1], turn_recv.at[k - 1], **member(k)
        ))
        for k in range(1, group)
    ]
    for d in range(3, fs_count):
        pass_weights(d)
    for copy in owned_copies + turn_copies:

        copy.wait_recv()
    for copy in sent:
        copy.wait_send()
    settle_weights()


def finish(*refs):
    sources, targets, inside, made = refs[:13], refs[13:23], refs[23:36], refs[36:46]
    load_sem, store_sem = refs[46:]
    (
        direction, owned, clip, all_value, all_output, basis_value, basis_output,
        weight_value, weight_output, first_value, second_value, first_output, second_output,
    ) = inside
    fs_count = all_value.shape[0]
    fs = lax.axis_index("fs")
    count = weight_value.shape[0]
    width = weight_value.shape[1]
    loads = [
        pltpu.make_async_copy(sources[i], inside[i], load_sem.at[i]) for i in range(len(inside))
    ]
    for i in (0, 5, 7, 6, 8, 3, 4, 1, 2, 9, 10, 11, 12):
        loads[i].start()
    stores = []

    def store(i, here=None):
        source, target = made[i], targets[i]
        if here is not None:
            source, target = source.at[here], target.at[here]
        copy = pltpu.make_async_copy(source, target, store_sem.at[len(stores)])
        copy.start()
        stores.append(copy)

    def ready(*which):
        for i in which:
            loads[i].wait()

    across = (((1,), (1,)), ((), ()))
    mine = pl.ds(pl.multiple_of(fs * count, count), count)
    ready(0, 5)
    turn_value = direction[:, 0].reshape(RANK, width)
    turn_output = direction[:, 1].reshape(RANK, width).astype(jnp.float32).T.astype(jnp.bfloat16)

    def value_step(rows_here):
        return jnp.dot(basis_value[rows_here], turn_value, preferred_element_type=jnp.float32)

    def output_step(rows_here):
        return lax.dot_general(
            turn_output, basis_output[rows_here], across, preferred_element_type=jnp.float32
        )

    step = value_step(mine)
    made[0][...] = step
    store(0)
    ready(7)
    made[2][...] = weight_value[...] - learning_rate * step
    store(2)
    ready(6)
    step = output_step(mine)
    made[1][...] = step
    store(1)
    ready(8)
    made[3][...] = weight_output[...] - learning_rate * step
    store(3)
    ready(3)
    for f in range(fs_count):
        here = pl.ds(f * count, count)
        made[4][here] = (
            all_value[f].astype(jnp.float32) - learning_rate * value_step(here)
        ).astype(jnp.bfloat16)
        store(4, here)
    ready(4)
    for f in range(fs_count):
        here = pl.ds(f * count, count)
        made[5][:, here] = (
            all_output[f].astype(jnp.float32) - learning_rate * output_step(here)
        ).astype(jnp.bfloat16)
        store(5, (slice(None), here))
    ready(1, 2, 9, 10, 11, 12)
    scale = clip[:1, :1]
    for a, (first, second) in enumerate(
        ((first_value, second_value), (first_output, second_output))
    ):
        projected = owned[:, a].reshape(first.shape)
        new_first, new_second, _ = moments(projected, first[...], second[...], scale)
        made[6 + 2 * a][...] = new_first
        made[7 + 2 * a][...] = new_second
        store(6 + 2 * a)
        store(7 + 2 * a)
    for copy in stores:
        copy.wait()


def kernels(
    fs_count, rep_count, tp_count,
    saved_hidden, grad_value, saved_mixed, grad_output, basis_value, basis_output,
    weight_value, weight_output, first_value, second_value, first_output, second_output,
):
    group = fs_count * rep_count
    tokens, model = saved_hidden.shape
    count, width = weight_value.shape
    rank = basis_value.shape[1]
    rows = rank // group
    f32, bf16 = jnp.float32, jnp.bfloat16
    shape = jax.ShapeDtypeStruct
    dma = pltpu.SemaphoreType.DMA
    anywhere = pl.BlockSpec(memory_space=pl.ANY)
    in_vmem = pl.BlockSpec(memory_space=pltpu.VMEM)
    direction, owned, clip, all_value, all_output = pl.pallas_call(
        functools.partial(exchange, fs_count, rep_count, tp_count),
        out_shape=(
            shape((group, 2, rows, width), bf16),
            shape((rep_count, 2, rows, width), f32),
            shape((8, 128), f32),
            shape((fs_count, count, width), bf16),
            shape((fs_count, width, count), bf16),
        ),
        in_specs=[anywhere] * 12,
        out_specs=(in_vmem,) * 5,
        scratch_shapes=[
            pltpu.VMEM((2, tokens, model), bf16),
            pltpu.VMEM((2, tokens, width), bf16),
            pltpu.VMEM((2, model, rank), bf16),
            pltpu.VMEM((count, width), f32),
            pltpu.VMEM((width, count), f32),
            pltpu.VMEM((4, rows, width), f32),
            pltpu.VMEM((2, group, rows, width), f32),
            pltpu.VMEM((2, group - 1, rows, width), f32),
            pltpu.VMEM((group * tp_count, 1, 128), f32),
            dma((14,)),
            dma((2, 2, fs_count - 1)), dma((2, 2, fs_count - 1)),
            dma((2, 2, fs_count - 1, rep_count - 1)), dma((2, 2, fs_count - 1, rep_count - 1)),
            dma((2, group - 1)), dma((2, group - 1)),
            dma((group * tp_count - 1,)), dma((group * tp_count - 1,)),
            dma((rep_count - 1,)), dma((rep_count - 1,)),
            dma((group - 1,)), dma((group - 1,)),
        ],
        compiler_params=pltpu.CompilerParams(
            collective_id=0, has_side_effects=True, vmem_limit_bytes=60 * 1024 * 1024
        ),
        name="exchange",
    )(
        saved_hidden, grad_value, saved_mixed, grad_output, basis_value, basis_output,
        weight_value, weight_output, first_value, second_value, first_output, second_output,
    )
    moment = shape(first_value.shape, f32)
    operands = (
        direction, owned, clip, all_value, all_output, basis_value, basis_output,
        weight_value, weight_output, first_value, second_value, first_output, second_output,
    )
    results = (
        shape((count, width), f32), shape((width, count), f32),
        shape((count, width), f32), shape((width, count), f32),
        shape((model, width), bf16), shape((width, model), bf16),
        moment, moment, moment, moment,
    )
    return pl.pallas_call(
        finish,
        out_shape=results,
        in_specs=[anywhere] * len(operands),
        out_specs=(anywhere,) * len(results),
        scratch_shapes=[pltpu.VMEM(x.shape, x.dtype) for x in operands + results]
        + [dma((len(operands),)), dma((len(results) - 2 + 2 * fs_count,))],
        compiler_params=pltpu.CompilerParams(vmem_limit_bytes=60 * 1024 * 1024),
        name="finish",
    )(*operands)


def solution(mesh):
    fs_count, rep_count, tp_count = mesh.shape["fs"], mesh.shape["rep"], mesh.shape["tp"]
    whole_tiles = RANK % (16 * fs_count * rep_count) == 0
    body = functools.partial(kernels, fs_count, rep_count, tp_count) if whole_tiles else local
    return jax.shard_map(
        body,
        mesh=mesh,
        in_specs=(
            P(("fs", "rep"), None),
            P(("fs", "rep"), "tp"),
            P(("fs", "rep"), "tp"),
            P(("fs", "rep"), None),
            P(),
            P(),
            P("fs", "tp"),
            P("tp", "fs"),
            P("fs", "tp"),
            P("fs", "tp"),
            P("fs", "tp"),
            P("fs", "tp"),
        ),
        out_specs=(
            P("fs", "tp"),
            P("tp", "fs"),
            P("fs", "tp"),
            P("tp", "fs"),
            P(None, "tp"),
            P("tp", None),
            P("fs", "tp"),
            P("fs", "tp"),
            P("fs", "tp"),
            P("fs", "tp"),
        ),
        check_vma=False,
    )
```

profile of v0, /device:TPU:0, one launch (start us, length us, event | category | flops | bytes accessed | tf_op | source)
XLA Modules:
  0.0 43.0 jit_solution(16070069158896096645)
XLA Ops:
  0.6 38.5 %exchange.1 = (bf16[8,2,16,256]{3,2,1,0:T(8,128)(2,1)}, f32[2,2,16,256]{3,2,1,0:T(8,128)}, f32[8,128]{1,0:T(8,128)}, bf16[4,512,256]{2,1,0:T(8,128)(2,1)}, bf16[4,256,512]{2,1,0:T(8,128)(2,1)}) custom-call(bf16[896,2048]{1,0:T(8,128)(2,1)} %hidden.1, bf16[896,256]{1,0:T(8,128)(2,1)} %grad_value.1, bf16[896,256]{1,0:T(8,128)(2,1)} %mixed.1, ...), custom_call_target="tpu_custom_call" | custom-call | tf_op jit(solution)/shard_map/exchange/pallas_call | solution.py:445
  39.2 3.9 %finish.1 = (f32[512,256]{1,0:T(8,128)}, f32[256,512]{1,0:T(8,128)}, f32[512,256]{1,0:T(8,128)}, f32[256,512]{1,0:T(8,128)}, bf16[2048,256]{1,0:T(8,128)(2,1)}, ...) custom-call(bf16[8,2,16,256]{3,2,1,0:T(8,128)(2,1)} %get-tuple-eleme, ...), custom_call_target="tpu_custom_call" | custom-call | tf_op jit(solution)/shard_map/finish/pallas_call | solution.py:493
where the time goes:
time: 43.2 us; the launch traced here: 43 us
  Pallas kernels  42.4 us (98%)
  between operations  0.65 us (2%)
    pallas_call x1, Pallas kernels, kernels(): pl.pallas_call(functools.partial(exchange, fs_count, rep_count, tp_count)...  38.5 us
    pallas_call x1, Pallas kernels, kernels(): pl.pallas_call(finish, out_shape=results, in_specs=[anywhere] * len(opera...  3.88 us

commit v1 on v0

v1 whole, which is shorter than its diff:
```python
import functools
import jax
import jax.numpy as jnp
from jax import lax
from jax.experimental import pallas as pl
from jax.experimental.pallas import tpu as pltpu
from jax.sharding import PartitionSpec as P

AW = 1024
RANK = 128

TOKEN_PIECES = 4
PIECES = 2
EXTRA = 1
EARLY = 3
VMEM_LIMIT = 59 * 1024 * 1024


first_decay = 0.8
second_decay = 0.9
learning_rate = 0.02
norm_epsilon = 1e-06
contract_leading = (((0,), (0,)), ((), ()))


def moments(projected, first_old, second_old, clip_factor):
    scaled = clip_factor * projected
    first_new = first_decay * first_old + (1.0 - first_decay) * scaled
    second_new = second_decay * second_old + (1.0 - second_decay) * scaled * scaled
    return (first_new, second_new, first_new / jnp.sqrt(second_new))


def split_product(reduced, other):
    upper = reduced.astype(jnp.bfloat16)
    lower = (reduced - upper.astype(jnp.float32)).astype(jnp.bfloat16)
    rank_count = reduced.shape[1]
    stacked = jnp.concatenate([upper, lower], axis=1)
    both = lax.dot_general(stacked, other, contract_leading, preferred_element_type=jnp.float32)
    return both[:rank_count] + both[rank_count:]


def local(
    saved_hidden,
    grad_value,
    saved_mixed,
    grad_output,
    basis_value,
    basis_output,
    weight_value,
    weight_output,
    first_value,
    second_value,
    first_output,
    second_output,
):
    row_count = weight_value.shape[0]
    moment_count = first_value.shape[0]
    fs_index = lax.axis_index("fs")
    row_first = fs_index * row_count
    moment_first = fs_index * moment_count
    value_basis_rows = lax.dynamic_slice_in_dim(basis_value, row_first, row_count, 0).astype(
        jnp.float32
    )
    output_basis_rows = lax.dynamic_slice_in_dim(basis_output, row_first, row_count, 0).astype(
        jnp.float32
    )
    reduced_hidden = jnp.dot(saved_hidden, basis_value, preferred_element_type=jnp.float32)
    reduced_output = jnp.dot(grad_output, basis_output, preferred_element_type=jnp.float32)
    part_value = split_product(reduced_hidden, grad_value)
    part_output = split_product(reduced_output, saved_mixed)
    projected_value, projected_output = lax.psum((part_value, part_output), ("fs", "rep"))
    local_squares = jnp.sum(projected_value * projected_value) + jnp.sum(
        projected_output * projected_output
    )
    total_squares = lax.psum(local_squares, "tp")
    mean_square = total_squares / (2 * RANK * AW)
    clip_factor = jnp.minimum(1.0, 1.0 / jnp.sqrt(mean_square + norm_epsilon))
    value_slice = lax.dynamic_slice_in_dim(projected_value, moment_first, moment_count, 0)
    output_slice = lax.dynamic_slice_in_dim(projected_output, moment_first, moment_count, 0)
    new_first_value, new_second_value, value_direction_rows = moments(
        value_slice, first_value, second_value, clip_factor
    )
    new_first_output, new_second_output, output_direction_rows = moments(
        output_slice, first_output, second_output, clip_factor
    )
    direction_value, direction_output = (
        lax.all_gather(value_direction_rows, "fs", axis=0, tiled=True),
        lax.all_gather(output_direction_rows, "fs", axis=0, tiled=True),
    )
    step_value = jnp.dot(value_basis_rows, direction_value, precision=lax.Precision.HIGHEST)
    step_output = jnp.dot(output_basis_rows, direction_output, precision=lax.Precision.HIGHEST).T
    new_weight_value = weight_value - learning_rate * step_value
    new_weight_output = weight_output - learning_rate * step_output
    copy_value, copy_output = (
        lax.all_gather(new_weight_value.astype(jnp.bfloat16), "fs", axis=0, tiled=True),
        lax.all_gather(new_weight_output.astype(jnp.bfloat16), "fs", axis=1, tiled=True),
    )
    return (
        step_value,
        step_output,
        new_weight_value,
        new_weight_output,
        copy_value,
        copy_output,
        new_first_value,
        new_second_value,
        new_first_output,
        new_second_output,
    )


MESH = pl.DeviceIdType.MESH


def remote(src, dst, send, recv, **where):
    return pltpu.make_async_remote_copy(
        src_ref=src, dst_ref=dst, send_sem=send, recv_sem=recv, device_id=where, device_id_type=MESH
    )


def exchange(
    fs_count, rep_count, tp_count,
    hidden, grad_value, mixed, grad_output, basis_value, basis_output, weight_value, weight_output,
    first_value, second_value, first_output, second_output,
    step_value, step_output, new_value, new_output, copy_value, copy_output,
    new_first_value, new_second_value, new_first_output, new_second_output,
    tokens_in, thin_in, basis_in, value_in, output_in, moment_in, all_value, all_output,
    part, part_sent, landed, squares_all, owned, direction,
    load_sem, near_send, near_recv, side_send, side_recv, part_send, part_recv,
    square_send, square_recv, owned_send, owned_recv, turn_send, turn_recv, ready,
):
    group = fs_count * rep_count
    everyone = group * tp_count
    fs, rep, tp = lax.axis_index("fs"), lax.axis_index("rep"), lax.axis_index("tp")
    me = fs * rep_count + rep
    tokens = hidden.shape[0]
    count, width = value_in.shape
    rows = part.shape[2]
    piece = tokens // TOKEN_PIECES
    f32, bf16 = jnp.float32, jnp.bfloat16

    loads = []

    def load(source, target):
        copy = pltpu.make_async_copy(source, target, load_sem.at[len(loads)])
        copy.start()
        loads.append(copy)
        return copy

    weight_loads = [load(weight_value, value_in), load(weight_output, output_in)]
    stream_loads = []
    for a, (big, thin, basis) in enumerate(
        ((hidden, grad_value, basis_value), (grad_output, mixed, basis_output))
    ):
        first = [load(basis, basis_in.at[a]), load(thin, thin_in.at[a])]
        blocks = [
            load(big.at[pl.ds(c * piece, piece)], tokens_in.at[a, pl.ds(c * piece, piece)])
            for c in range(TOKEN_PIECES)
        ]
        stream_loads.append((first, blocks))
    moment_loads = [
        load(source, moment_in.at[i])
        for i, source in enumerate((first_value, first_output, second_value, second_output))
    ]

    def member(k):
        other = lax.rem(me + k, group)
        return {"fs": other // rep_count, "rep": lax.rem(other, rep_count)}

    def anyone(k):
        other = lax.rem(me * tp_count + tp + k, everyone)
        at = other // tp_count
        return {"fs": at // rep_count, "rep": lax.rem(at, rep_count), "tp": lax.rem(other, tp_count)}

    def signal(sem, **where):
        pl.semaphore_signal(sem, inc=1, device_id=where, device_id_type=MESH)

    has_next = (fs > 0, fs < fs_count - 1)

    def signal_beside(sem):
        for there, step in zip(has_next, (-1, 1)):
            @pl.when(there)
            def _():
                signal(sem, fs=fs + step)

    beside = has_next[0].astype(jnp.int32) + has_next[1].astype(jnp.int32)
    barrier = pltpu.get_barrier_semaphore()
    signal_beside(barrier)
    for j in range(1, rep_count):
        signal(barrier, rep=lax.rem(rep + j, rep_count))
    for j in range(1, tp_count):
        signal(barrier, tp=lax.rem(tp + j, tp_count))

    for copy in weight_loads:
        copy.wait()
    all_value[fs] = value_in[...].astype(bf16)
    all_output[fs] = output_in[...].astype(bf16)
    pl.semaphore_wait(barrier, beside + (rep_count - 1 + tp_count - 1))
    for j in range(1, rep_count):
        signal(ready.at[0], rep=lax.rem(rep + j, rep_count))

    def meet(k):
        if k == 0:
            pl.semaphore_wait(ready.at[0], rep_count - 1)
        else:
            pl.semaphore_wait(ready.at[k], beside)
        if k + 1 < fs_count:
            signal_beside(ready.at[k + 1])

    buffers = (all_value, all_output)
    spans = (count // (rep_count * PIECES), width // (rep_count * PIECES))

    def spot(f, s, a, q):
        owner = rep if s == 0 else lax.rem(rep + s, rep_count)
        start = pl.multiple_of((owner * PIECES + q) * spans[a], spans[a])
        return buffers[a].at[f, pl.ds(start, spans[a])]

    own_items = [(0, a, q) for a in range(2) for q in range(PIECES)]
    far_items = [(1, 1, q) for q in range(EXTRA)]
    rest_items = [(1, a, q) for a in range(2) for q in range(PIECES) if (1, a, q) not in far_items]

    def both(x, y):
        return jnp.logical_and(x, y)

    def onward(way):
        return has_next[1] if way == 0 else has_next[0]

    def reaches(way, d):
        return fs >= d if way == 0 else fs + d < fs_count

    def outer(way, d):
        return fs == d if way == 0 else fs == fs_count - 1 - d

    def comes(way, d, item):
        if item in own_items:
            return reaches(way, d)
        if item in far_items or d <= 1:
            return outer(way, d)
        return None

    def goes(way, d, item):
        if item in rest_items and d > 0:
            return None
        there = comes(way, d, item)
        return both(onward(way), there)

    def crosses(way, d, item):
        _, a, q = item
        if d == 1 or (1, a, q) in far_items:
            if d == fs_count - 1:
                return None
            return both(reaches(way, d), jnp.logical_not(outer(way, d)))
        return reaches(way, d)

    def step_of(way):
        return 1 if way == 0 else -1

    def hop(way, d, item):
        s, a, q = item
        block = spot(fs - step_of(way) * d, s, a, q)
        at = (way, d, s, a, q)
        return remote(block, block, near_send.at[at], near_recv.at[at], fs=fs + step_of(way))

    def arrival(way, d, item):
        s, a, q = item
        block = spot(fs - step_of(way) * d, s, a, q)
        at = (way, d - 1, s, a, q)
        return remote(block, block, near_send.at[at], near_recv.at[at], fs=fs - step_of(way))

    def across(way, d, item, s=0):
        _, a, q = item
        block = spot(fs - step_of(way) * d, s, a, q)
        at = (way, d - 1, a, q)
        return remote(
            block, block, side_send.at[at], side_recv.at[at], rep=lax.rem(rep + 1, rep_count)
        )

    later = []

    def send_when(there, make):
        @pl.when(there)
        def _():
            make().start()

        later.append((there, make))

    def send_own(items):
        for item in items:
            for way in range(2):
                there = goes(way, 0, item)
                send_when(there, functools.partial(hop, way, 0, item))

    def pass_on(d, items):
        for item in items:
            for way in range(2):
                there = comes(way, d, item)
                if there is None:
                    continue

                @pl.when(there)
                def _():
                    arrival(way, d, item).wait_recv()

                if d < fs_count - 1:
                    onwards = goes(way, d, item)
                    if onwards is not None:
                        send_when(onwards, functools.partial(hop, way, d, item))
                if item in own_items:
                    over = crosses(way, d, item)
                    if over is not None:
                        send_when(over, functools.partial(across, way, d, item))

    sent = []

    def send(copy):
        copy.start()
        sent.append(copy)
        return copy

    parts = []

    def send_part(a, total):
        part[a] = total.reshape(group, rows, width)
        part_sent[a] = total.astype(bf16).reshape(group, rows, width)
        for k in range(1, group):
            other = lax.rem(me + k, group)
            parts.append(send(remote(
                part_sent.at[a, other], landed.at[a, k - 1],
                part_send.at[a, k - 1], part_recv.at[a, k - 1], **member(k),
            )))

    send_own(own_items[:EARLY])
    totals = [None, None]
    pending = None

    def finish_piece(a, c, reduced):
        product = split_product(reduced, thin_in[a, pl.ds(c * piece, piece)])
        totals[a] = product if totals[a] is None else totals[a] + product

    met = 0
    for a in range(2):
        first, blocks = stream_loads[a]
        for copy in first:
            copy.wait()
        for c in range(TOKEN_PIECES):
            blocks[c].wait()
            reduced = jnp.dot(
                tokens_in[a, pl.ds(c * piece, piece)], basis_in[a], preferred_element_type=f32
            )
            if pending is not None:
                finish_piece(*pending)
                if pending[1] == TOKEN_PIECES - 1:
                    while met < fs_count:
                        meet(met)
                        met += 1
                    send_part(pending[0], totals[pending[0]])
                    send_own(own_items[EARLY:])
            pending = (a, c, reduced)
            if met < fs_count:
                meet(met)
                met += 1
    finish_piece(*pending)
    send_part(1, totals[1])
    send_own(far_items + rest_items)

    pass_on(1, own_items + far_items)
    for copy in parts:
        copy.wait_recv()
    squares = jnp.zeros((rows, width), f32)
    for a in range(2):
        summed = part[a, me]
        for k in range(group - 1):
            summed = summed + landed[a, k].astype(f32)
        owned[rep, a] = summed
        squares = squares + summed * summed
    place = me * tp_count + tp
    squares_all[place] = jnp.full(squares_all.shape[1:], jnp.sum(squares), f32)
    square_copies = [
        send(remote(
            squares_all.at[place], squares_all.at[place],
            square_send.at[k - 1], square_recv.at[k - 1], **anyone(k),
        ))
        for k in range(1, everyone)
    ]
    owned_copies = [
        send(remote(
            owned.at[rep], owned.at[rep], owned_send.at[j - 1], owned_recv.at[j - 1],
            rep=lax.rem(rep + j, rep_count),
        ))
        for j in range(1, rep_count)
    ]
    for d in range(2, fs_count - 1):
        pass_on(d, own_items)
    for copy in moment_loads:
        copy.wait()
    for copy in square_copies:
        copy.wait_recv()
    mean_square = jnp.sum(squares_all[...], axis=0) / (2 * RANK * AW)
    factor = jnp.minimum(1.0, 1.0 / jnp.sqrt(mean_square + norm_epsilon))
    scale = factor[:1, :1]
    mine_rows = pl.ds(pl.multiple_of(rep * rows, rows), rows)
    for a in range(2):
        _, _, turned = moments(
            owned[rep, a], moment_in[a, mine_rows], moment_in[2 + a, mine_rows], scale
        )
        direction[me, a] = turned.astype(bf16)
    turn_copies = [
        send(remote(
            direction.at[me], direction.at[me], turn_send.at[k - 1], turn_recv.at[k - 1], **member(k)
        ))
        for k in range(1, group)
    ]
    for d in range(2, fs_count - 1):
        pass_on(d, far_items)
    pass_on(fs_count - 1, own_items + far_items)
    for copy in owned_copies:
        copy.wait_recv()
    firsts, seconds = (new_first_value, new_first_output), (new_second_value, new_second_output)
    for a in range(2):
        projected = owned[:, a].reshape(firsts[a].shape)
        firsts[a][...], seconds[a][...], _ = moments(
            projected, moment_in[a], moment_in[2 + a], scale
        )
    for copy in turn_copies:
        copy.wait_recv()

    over = (((1,), (1,)), ((), ()))
    turn_value = direction[:, 0].reshape(RANK, width)
    turn_output = direction[:, 1].reshape(RANK, width).astype(f32).T.astype(bf16)

    def here(f):
        return pl.ds(pl.multiple_of(f * count, count), count)

    def value_step(f):
        return jnp.dot(basis_in[0, here(f)], turn_value, preferred_element_type=f32)

    def output_step(f):
        return lax.dot_general(turn_output, basis_in[1, here(f)], over, preferred_element_type=f32)

    def move(weight, step):
        return (weight.astype(f32) - learning_rate * step).astype(bf16)

    step = value_step(fs)
    step_value[...] = step
    new_value[...] = value_in[...] - learning_rate * step
    copy_value[here(fs)] = move(all_value[fs], step)
    step = output_step(fs)
    step_output[...] = step
    new_output[...] = output_in[...] - learning_rate * step
    copy_output[:, here(fs)] = move(all_output[fs], step)

    for d in range(1, fs_count):
        for a in range(2):
            for way in range(2):
                if d == 1:
                    pass_on_rest = [item for item in rest_items if item[1] == a]
                    for item in pass_on_rest:
                        @pl.when(comes(way, d, item))
                        def _():
                            arrival(way, d, item).wait_recv()
                for item in own_items:
                    if item[1] == a:
                        there = crosses(way, d, item)
                        if there is not None:
                            @pl.when(there)
                            def _():
                                across(way, d, item, 1).wait_recv()

                @pl.when(reaches(way, d))
                def _():
                    f = fs - step_of(way) * d
                    if a == 0:
                        copy_value[here(f)] = move(all_value[f], value_step(f))
                    else:
                        copy_output[:, here(f)] = move(all_output[f], output_step(f))

    for copy in sent:
        copy.wait_send()
    for there, make in later:
        @pl.when(there)
        def _():
            make().wait_send()


def finish(*refs):
    made = len(refs) // 2
    sources, targets, sem = refs[:made], refs[made : 2 * made], refs[-1]
    copies = [
        pltpu.make_async_copy(sources[i], targets[i], sem.at[i]) for i in range(made)
    ]
    for copy in copies:
        copy.start()
    for copy in copies:
        copy.wait()


def kernels(
    fs_count, rep_count, tp_count,
    saved_hidden, grad_value, saved_mixed, grad_output, basis_value, basis_output,
    weight_value, weight_output, first_value, second_value, first_output, second_output,
):
    group = fs_count * rep_count
    tokens, model = saved_hidden.shape
    count, width = weight_value.shape
    rank = basis_value.shape[1]
    rows = rank // group
    f32, bf16 = jnp.float32, jnp.bfloat16
    dma = pltpu.SemaphoreType.DMA
    anywhere = pl.BlockSpec(memory_space=pl.ANY)
    in_vmem = pl.BlockSpec(memory_space=pltpu.VMEM)
    moment = (first_value.shape, f32)
    results = (
        ((count, width), f32), ((width, count), f32), ((count, width), f32), ((width, count), f32),
        ((model, width), bf16), ((width, model), bf16), moment, moment, moment, moment,
    )
    hops = (2, fs_count - 1, rep_count, 2, PIECES)
    sides = (2, fs_count - 1, 2, PIECES)
    made = pl.pallas_call(
        functools.partial(exchange, fs_count, rep_count, tp_count),
        out_shape=tuple(pltpu.VMEM(*x) for x in results),
        in_specs=[anywhere] * 12,
        out_specs=(in_vmem,) * len(results),
        scratch_shapes=[
            pltpu.VMEM((2, tokens, model), bf16),
            pltpu.VMEM((2, tokens, width), bf16),
            pltpu.VMEM((2, model, rank), bf16),
            pltpu.VMEM((count, width), f32),
            pltpu.VMEM((width, count), f32),
            pltpu.VMEM((4,) + first_value.shape, f32),
            pltpu.VMEM((fs_count, count, width), bf16),
            pltpu.VMEM((fs_count, width, count), bf16),
            pltpu.VMEM((2, group, rows, width), f32),
            pltpu.VMEM((2, group, rows, width), bf16),
            pltpu.VMEM((2, group - 1, rows, width), bf16),
            pltpu.VMEM((group * tp_count, 1, 128), f32),
            pltpu.VMEM((rep_count, 2, rows, width), f32),
            pltpu.VMEM((group, 2, rows, width), bf16),
            dma((10 + 2 * TOKEN_PIECES,)),
            dma(hops), dma(hops), dma(sides), dma(sides),
            dma((2, group - 1)), dma((2, group - 1)),
            dma((group * tp_count - 1,)), dma((group * tp_count - 1,)),
            dma((rep_count - 1,)), dma((rep_count - 1,)),
            dma((group - 1,)), dma((group - 1,)),
            pltpu.SemaphoreType.REGULAR((fs_count,)),
        ],
        compiler_params=pltpu.CompilerParams(
            collective_id=0, has_side_effects=True, vmem_limit_bytes=VMEM_LIMIT
        ),
        name="exchange",
    )(
        saved_hidden, grad_value, saved_mixed, grad_output, basis_value, basis_output,
        weight_value, weight_output, first_value, second_value, first_output, second_output,
    )
    return pl.pallas_call(
        finish,
        out_shape=tuple(jax.ShapeDtypeStruct(*x) for x in results),
        in_specs=[anywhere] * len(results),
        out_specs=(anywhere,) * len(results),
        scratch_shapes=[dma((len(results),))],
        compiler_params=pltpu.CompilerParams(vmem_limit_bytes=1024 * 1024),
        name="finish",
    )(*made)


def solution(mesh):
    fs_count, rep_count, tp_count = mesh.shape["fs"], mesh.shape["rep"], mesh.shape["tp"]
    whole_tiles = RANK % (16 * fs_count * rep_count) == 0 and rep_count == 2 and fs_count > 2
    body = functools.partial(kernels, fs_count, rep_count, tp_count) if whole_tiles else local
    return jax.shard_map(
        body,
        mesh=mesh,
        in_specs=(
            P(("fs", "rep"), None),
            P(("fs", "rep"), "tp"),
            P(("fs", "rep"), "tp"),
            P(("fs", "rep"), None),
            P(),
            P(),
            P("fs", "tp"),
            P("tp", "fs"),
            P("fs", "tp"),
            P("fs", "tp"),
            P("fs", "tp"),
            P("fs", "tp"),
        ),
        out_specs=(
            P("fs", "tp"),
            P("tp", "fs"),
            P("fs", "tp"),
            P("tp", "fs"),
            P(None, "tp"),
            P("tp", None),
            P("fs", "tp"),
            P("fs", "tp"),
            P("fs", "tp"),
            P("fs", "tp"),
        ),
        check_vma=False,
    )
```

time: 43.2 us -> 36.7 us (0.85)
  Pallas kernels: 42.4 us -> 35.9 us
    pallas_call x1, Pallas kernels: 38.5 us -> 33.8 us  [kernels(): pl.pallas_call(functools.partial(exchange, fs_count, rep_count, tp_count)...]
    pallas_call x1, Pallas kernels: 3.88 us -> 2.12 us  [kernels(): pl.pallas_call(finish, out_shape=tuple((jax.ShapeDtypeStruct(*x) for x in...]
where the time goes in v1:
time: 36.7 us; the launch traced here: 36.5 us
  Pallas kernels  35.9 us (98%)
  between operations  0.66 us (2%)
    pallas_call x1, Pallas kernels, kernels(): pl.pallas_call(functools.partial(exchange, fs_count, rep_count, tp_count)...  33.8 us
    pallas_call x1, Pallas kernels, kernels(): pl.pallas_call(finish, out_shape=tuple((jax.ShapeDtypeStruct(*x) for x in...  2.12 us

profile of v1, /device:TPU:0, one launch (start us, length us, event | category | flops | bytes accessed | tf_op | source)
XLA Modules:
  0.0 36.5 jit_solution(13711946531731678184)
XLA Ops:
  0.6 33.8 %exchange.1 = (f32[512,256]{1,0:T(8,128)S(1)}, f32[256,512]{1,0:T(8,128)S(1)}, f32[512,256]{1,0:T(8,128)S(1)}, f32[256,512]{1,0:T(8,128)S(1)}, bf16[2048,256]{1,...) custom-call(bf16[896,2048]{1,0:T(8,128)(2,1)} %hidden.1, ...), custom_call_target="tpu_custom_call" | custom-call | tf_op jit(solution)/shard_map/exchange/pallas_call | solution.py:518
  34.4 2.1 %finish.1 = (f32[512,256]{1,0:T(8,128)}, f32[256,512]{1,0:T(8,128)}, f32[512,256]{1,0:T(8,128)}, f32[256,512]{1,0:T(8,128)}, bf16[2048,256]{1,0:T(8,128)(2,1)}, ...) custom-call(f32[512,256]{1,0:T(8,128)S(1)} %get-tuple-element.20.ref, ...), custom_call_target="tpu_custom_call" | custom-call | tf_op jit(solution)/shard_map/finish/pallas_call | solution.py:554

commit v2 on v1

--- a/solution.py
+++ b/solution.py
@@ -12,8 +12,12 @@
 TOKEN_PIECES = 4
 PIECES = 2
 EXTRA = 1
-EARLY = 3
+EARLY = 4
+AHEAD = 4
+LATE = 4
 VMEM_LIMIT = 59 * 1024 * 1024
+MEETINGS = 3
+MEET_AT = (1, 3, 5)
 
 
 first_decay = 0.8
@@ -122,22 +126,43 @@
     fs_count, rep_count, tp_count,
     hidden, grad_value, mixed, grad_output, basis_value, basis_output, weight_value, weight_output,
     first_value, second_value, first_output, second_output,
-    step_value, step_output, new_value, new_output, copy_value, copy_output,
-    new_first_value, new_second_value, new_first_output, new_second_output,
+    *refs,
+):
+    targets, made, refs = refs[:10], refs[10:20], refs[20:]
+    (
     tokens_in, thin_in, basis_in, value_in, output_in, moment_in, all_value, all_output,
     part, part_sent, landed, squares_all, owned, direction,
-    load_sem, near_send, near_recv, side_send, side_recv, part_send, part_recv,
-    square_send, square_recv, owned_send, owned_recv, turn_send, turn_recv, ready,
-):
+    load_sem, sent_sem, near_recv, side_recv, part_recv, square_recv, owned_recv, turn_recv,
+    ready, store_sem,
+    ) = refs
+    step_value, step_output, new_value, new_output, copy_value, copy_output = made[:6]
     group = fs_count * rep_count
     everyone = group * tp_count
     fs, rep, tp = lax.axis_index("fs"), lax.axis_index("rep"), lax.axis_index("tp")
     me = fs * rep_count + rep
+    at_end = jnp.logical_or(fs == 0, fs == fs_count - 1)
     tokens = hidden.shape[0]
     count, width = value_in.shape
     rows = part.shape[2]
     piece = tokens // TOKEN_PIECES
     f32, bf16 = jnp.float32, jnp.bfloat16
+
+    stores = []
+
+    def store(i, here=None, there=None):
+        def make():
+            source, target = made[i], targets[i]
+            if here is not None:
+                source, target = source.at[here], target.at[here]
+            return pltpu.make_async_copy(source, target, store_sem)
+
+        if there is None:
+            make().start()
+        else:
+            @pl.when(there)
+            def _():
+                make().start()
+        stores.append((there, make))
 
     loads = []
 
@@ -191,23 +216,27 @@
     for j in range(1, tp_count):
         signal(barrier, tp=lax.rem(tp + j, tp_count))
 
+    pl.semaphore_wait(barrier, beside + (rep_count - 1 + tp_count - 1))
+    signal_beside(ready.at[0])
+    for j in range(1, rep_count):
+        signal(ready.at[0], rep=lax.rem(rep + j, rep_count))
+    inputs, buffers = (value_in, output_in), (all_value, all_output)
+
+    def cast(owner_rep):
+        for a in range(2):
+            share = inputs[a].shape[0] // rep_count
+            here = pl.ds(pl.multiple_of(owner_rep * share, share), share)
+            buffers[a][fs, here] = inputs[a][here].astype(bf16)
+
     for copy in weight_loads:
         copy.wait()
-    all_value[fs] = value_in[...].astype(bf16)
-    all_output[fs] = output_in[...].astype(bf16)
-    pl.semaphore_wait(barrier, beside + (rep_count - 1 + tp_count - 1))
-    for j in range(1, rep_count):
-        signal(ready.at[0], rep=lax.rem(rep + j, rep_count))
+    cast(rep)
 
     def meet(k):
-        if k == 0:
-            pl.semaphore_wait(ready.at[0], rep_count - 1)
-        else:
-            pl.semaphore_wait(ready.at[k], beside)
-        if k + 1 < fs_count:
+        pl.semaphore_wait(ready.at[k], beside + (rep_count - 1 if k == 0 else 0))
+        if k + 1 < MEETINGS:
             signal_beside(ready.at[k + 1])
 
-    buffers = (all_value, all_output)
     spans = (count // (rep_count * PIECES), width // (rep_count * PIECES))
 
     def spot(f, s, a, q):
@@ -255,25 +284,28 @@
     def step_of(way):
         return 1 if way == 0 else -1
 
+    def slot(block, at):
+        return jnp.where(block < at, block, block - 1)
+
     def hop(way, d, item):
         s, a, q = item
-        block = spot(fs - step_of(way) * d, s, a, q)
-        at = (way, d, s, a, q)
-        return remote(block, block, near_send.at[at], near_recv.at[at], fs=fs + step_of(way))
+        f, to = fs - step_of(way) * d, fs + step_of(way)
+        block = spot(f, s, a, q)
+        return remote(block, block, sent_sem, near_recv.at[slot(f, to), s, a, q], fs=to)
 
     def arrival(way, d, item):
         s, a, q = item
-        block = spot(fs - step_of(way) * d, s, a, q)
-        at = (way, d - 1, s, a, q)
-        return remote(block, block, near_send.at[at], near_recv.at[at], fs=fs - step_of(way))
+        f = fs - step_of(way) * d
+        block = spot(f, s, a, q)
+        at = near_recv.at[slot(f, fs), s, a, q]
+        return remote(block, block, sent_sem, at, fs=fs - step_of(way))
 
     def across(way, d, item, s=0):
         _, a, q = item
-        block = spot(fs - step_of(way) * d, s, a, q)
-        at = (way, d - 1, a, q)
-        return remote(
-            block, block, side_send.at[at], side_recv.at[at], rep=lax.rem(rep + 1, rep_count)
-        )
+        f = fs - step_of(way) * d
+        block = spot(f, s, a, q)
+        at = side_recv.at[slot(f, fs), a, q]
+        return remote(block, block, sent_sem, at, rep=lax.rem(rep + 1, rep_count))
 
     later = []
 
@@ -290,12 +322,14 @@
                 there = goes(way, 0, item)
                 send_when(there, functools.partial(hop, way, 0, item))
 
-    def pass_on(d, items):
+    def pass_on(d, items, only=None):
         for item in items:
             for way in range(2):
                 there = comes(way, d, item)
                 if there is None:
                     continue
+                if only is not None:
+                    there = both(there, only)
 
                 @pl.when(there)
                 def _():
@@ -304,11 +338,18 @@
                 if d < fs_count - 1:
                     onwards = goes(way, d, item)
                     if onwards is not None:
+                        if only is not None:
+                            onwards = both(onwards, only)
                         send_when(onwards, functools.partial(hop, way, d, item))
                 if item in own_items:
                     over = crosses(way, d, item)
                     if over is not None:
+                        if only is not None:
+                            over = both(over, only)
                         send_when(over, functools.partial(across, way, d, item))
+
+    def arrived(ref, sem):
+        pltpu.make_async_copy(ref, ref, sem).wait()
 
     sent = []
 
@@ -316,20 +357,20 @@
         copy.start()
         sent.append(copy)
         return copy
-
-    parts = []
 
     def send_part(a, total):
         part[a] = total.reshape(group, rows, width)
         part_sent[a] = total.astype(bf16).reshape(group, rows, width)
         for k in range(1, group):
             other = lax.rem(me + k, group)
-            parts.append(send(remote(
+            send(remote(
                 part_sent.at[a, other], landed.at[a, k - 1],
-                part_send.at[a, k - 1], part_recv.at[a, k - 1], **member(k),
-            )))
+                sent_sem, part_recv.at[a], **member(k),
+            ))
 
     send_own(own_items[:EARLY])
+    for j in range(1, rep_count):
+        cast(lax.rem(rep + j, rep_count))
     totals = [None, None]
     pending = None
 
@@ -349,23 +390,19 @@
             )
             if pending is not None:
                 finish_piece(*pending)
-                if pending[1] == TOKEN_PIECES - 1:
-                    while met < fs_count:
-                        meet(met)
-                        met += 1
-                    send_part(pending[0], totals[pending[0]])
-                    send_own(own_items[EARLY:])
             pending = (a, c, reduced)
-            if met < fs_count:
+            if a * TOKEN_PIECES + c in MEET_AT:
                 meet(met)
                 met += 1
+                if met == MEETINGS:
+                    send_part(0, totals[0])
+                    send_own(own_items[EARLY:])
     finish_piece(*pending)
     send_part(1, totals[1])
     send_own(far_items + rest_items)
-
-    pass_on(1, own_items + far_items)
-    for copy in parts:
-        copy.wait_recv()
+    pass_on(1, own_items)
+    for a in range(2):
+        arrived(landed.at[a], part_recv.at[a])
     squares = jnp.zeros((rows, width), f32)
     for a in range(2):
         summed = part[a, me]
@@ -375,26 +412,25 @@
         squares = squares + summed * summed
     place = me * tp_count + tp
     squares_all[place] = jnp.full(squares_all.shape[1:], jnp.sum(squares), f32)
-    square_copies = [
+    for k in range(1, everyone):
         send(remote(
             squares_all.at[place], squares_all.at[place],
-            square_send.at[k - 1], square_recv.at[k - 1], **anyone(k),
+            sent_sem, square_recv, **anyone(k),
         ))
-        for k in range(1, everyone)
-    ]
     owned_copies = [
         send(remote(
-            owned.at[rep], owned.at[rep], owned_send.at[j - 1], owned_recv.at[j - 1],
+            owned.at[rep], owned.at[rep], sent_sem, owned_recv.at[j - 1],
             rep=lax.rem(rep + j, rep_count),
         ))
         for j in range(1, rep_count)
     ]
+    pass_on(1, far_items)
     for d in range(2, fs_count - 1):
-        pass_on(d, own_items)
+        pass_on(d, own_items[:AHEAD])
+        pass_on(d, own_items[AHEAD:], at_end)
     for copy in moment_loads:
         copy.wait()
-    for copy in square_copies:
-        copy.wait_recv()
+    arrived(squares_all.at[pl.ds(0, everyone - 1)], square_recv)
     mean_square = jnp.sum(squares_all[...], axis=0) / (2 * RANK * AW)
     factor = jnp.minimum(1.0, 1.0 / jnp.sqrt(mean_square + norm_epsilon))
     scale = factor[:1, :1]
@@ -404,25 +440,15 @@
             owned[rep, a], moment_in[a, mine_rows], moment_in[2 + a, mine_rows], scale
         )
         direction[me, a] = turned.astype(bf16)
-    turn_copies = [
+    for k in range(1, group):
         send(remote(
-            direction.at[me], direction.at[me], turn_send.at[k - 1], turn_recv.at[k - 1], **member(k)
+            direction.at[me], direction.at[me], sent_sem, turn_recv, **member(k)
         ))
-        for k in range(1, group)
-    ]
     for d in range(2, fs_count - 1):
+        pass_on(d, own_items[AHEAD:], jnp.logical_not(at_end))
         pass_on(d, far_items)
-    pass_on(fs_count - 1, own_items + far_items)
-    for copy in owned_copies:
-        copy.wait_recv()
-    firsts, seconds = (new_first_value, new_first_output), (new_second_value, new_second_output)
-    for a in range(2):
-        projected = owned[:, a].reshape(firsts[a].shape)
-        firsts[a][...], seconds[a][...], _ = moments(
-            projected, moment_in[a], moment_in[2 + a], scale
-        )
-    for copy in turn_copies:
-        copy.wait_recv()
+    pass_on(fs_count - 1, own_items[:LATE])
+    arrived(direction.at[pl.ds(0, group - 1)], turn_recv)
 
     over = (((1,), (1,)), ((), ()))
     turn_value = direction[:, 0].reshape(RANK, width)
@@ -442,37 +468,63 @@
 
     step = value_step(fs)
     step_value[...] = step
+    store(0)
     new_value[...] = value_in[...] - learning_rate * step
+    store(2)
     copy_value[here(fs)] = move(all_value[fs], step)
+    store(4, here(fs))
     step = output_step(fs)
     step_output[...] = step
+    store(1)
     new_output[...] = output_in[...] - learning_rate * step
+    store(3)
     copy_output[:, here(fs)] = move(all_output[fs], step)
-
-    for d in range(1, fs_count):
-        for a in range(2):
-            for way in range(2):
-                if d == 1:
-                    pass_on_rest = [item for item in rest_items if item[1] == a]
-                    for item in pass_on_rest:
+    store(5, (slice(None), here(fs)))
+
+    def settle(d, a):
+        for way in range(2):
+            if d == 1:
+                for item in rest_items:
+                    if item[1] == a:
                         @pl.when(comes(way, d, item))
                         def _():
                             arrival(way, d, item).wait_recv()
-                for item in own_items:
-                    if item[1] == a:
-                        there = crosses(way, d, item)
-                        if there is not None:
-                            @pl.when(there)
-                            def _():
-                                across(way, d, item, 1).wait_recv()
-
-                @pl.when(reaches(way, d))
-                def _():
-                    f = fs - step_of(way) * d
-                    if a == 0:
-                        copy_value[here(f)] = move(all_value[f], value_step(f))
-                    else:
-                        copy_output[:, here(f)] = move(all_output[f], output_step(f))
+            for item in own_items:
+                if item[1] == a:
+                    there = crosses(way, d, item)
+                    if there is not None:
+                        @pl.when(there)
+                        def _():
+                            across(way, d, item, 1).wait_recv()
+
+            f = fs - step_of(way) * d
+            at = here(f)
+            held_there = reaches(way, d)
+
+            @pl.when(held_there)
+            def _():
+                if a == 0:
+                    copy_value[at] = move(all_value[f], value_step(f))
+                else:
+                    copy_output[:, at] = move(all_output[f], output_step(f))
+
+            store(4 + a, at if a == 0 else (slice(None), at), held_there)
+
+    for a in range(2):
+        settle(1, a)
+    pass_on(fs_count - 1, own_items[LATE:] + far_items)
+
+    for copy in owned_copies:
+        copy.wait_recv()
+    for a in range(2):
+        made[6 + 2 * a][...], made[7 + 2 * a][...], _ = moments(
+            owned[:, a].reshape(moment_in.shape[1:]), moment_in[a], moment_in[2 + a], scale
+        )
+        store(6 + 2 * a)
+        store(7 + 2 * a)
+    for d in range(2, fs_count):
+        for a in range(2):
+            settle(d, a)
 
     for copy in sent:
         copy.wait_send()
@@ -480,6 +532,14 @@
         @pl.when(there)
         def _():
             make().wait_send()
+
+    for there, make in stores:
+        if there is None:
+            make().wait()
+        else:
+            @pl.when(there)
+            def _():
+                make().wait()
 
 
 def finish(*refs):
@@ -507,20 +567,18 @@
     f32, bf16 = jnp.float32, jnp.bfloat16
     dma = pltpu.SemaphoreType.DMA
     anywhere = pl.BlockSpec(memory_space=pl.ANY)
-    in_vmem = pl.BlockSpec(memory_space=pltpu.VMEM)
     moment = (first_value.shape, f32)
     results = (
         ((count, width), f32), ((width, count), f32), ((count, width), f32), ((width, count), f32),
         ((model, width), bf16), ((width, model), bf16), moment, moment, moment, moment,
     )
-    hops = (2, fs_count - 1, rep_count, 2, PIECES)
-    sides = (2, fs_count - 1, 2, PIECES)
     made = pl.pallas_call(
         functools.partial(exchange, fs_count, rep_count, tp_count),
         out_shape=tuple(pltpu.VMEM(*x) for x in results),
         in_specs=[anywhere] * 12,
-        out_specs=(in_vmem,) * len(results),
-        scratch_shapes=[
+        out_specs=(anywhere,) * len(results),
+        scratch_shapes=[pltpu.VMEM(*x) for x in results]
+        + [
             pltpu.VMEM((2, tokens, model), bf16),
             pltpu.VMEM((2, tokens, width), bf16),
             pltpu.VMEM((2, model, rank), bf16),
@@ -535,13 +593,10 @@
             pltpu.VMEM((group * tp_count, 1, 128), f32),
             pltpu.VMEM((rep_count, 2, rows, width), f32),
             pltpu.VMEM((group, 2, rows, width), bf16),
-            dma((10 + 2 * TOKEN_PIECES,)),
-            dma(hops), dma(hops), dma(sides), dma(sides),
-            dma((2, group - 1)), dma((2, group - 1)),
-            dma((group * tp_count - 1,)), dma((group * tp_count - 1,)),
-            dma((rep_count - 1,)), dma((rep_count - 1,)),
-            dma((group - 1,)), dma((group - 1,)),
-            pltpu.SemaphoreType.REGULAR((fs_count,)),
+            dma((10 + 2 * TOKEN_PIECES,)), dma,
+            dma((fs_count - 1, rep_count, 2, PIECES)), dma((fs_count - 1, 2, PIECES)),
+            dma((2,)), dma, dma((rep_count - 1,)), dma,
+            pltpu.SemaphoreType.REGULAR((MEETINGS,)), dma,
         ],
         compiler_params=pltpu.CompilerParams(
             collective_id=0, has_side_effects=True, vmem_limit_bytes=VMEM_LIMIT
@@ -564,7 +619,7 @@
 
 def solution(mesh):
     fs_count, rep_count, tp_count = mesh.shape["fs"], mesh.shape["rep"], mesh.shape["tp"]
-    whole_tiles = RANK % (16 * fs_count * rep_count) == 0 and rep_count == 2 and fs_count > 2
+    whole_tiles = rep_count == 2 and fs_count > 2 and RANK % (16 * fs_count * rep_count) == 0
     body = functools.partial(kernels, fs_count, rep_count, tp_count) if whole_tiles else local
     return jax.shard_map(
         body,

time: 36.7 us -> 34.5 us (0.940)
  Pallas kernels: 35.9 us -> 33.7 us
    pallas_call x1, Pallas kernels: 33.8 us -> 31.6 us  [kernels(): pl.pallas_call(functools.partial(exchange, fs_count, rep_count, tp_count)...]
where the time goes in v2:
time: 34.5 us; the launch traced here: 34.4 us
  Pallas kernels  33.7 us (98%)
  between operations  0.66 us (2%)
    pallas_call x1, Pallas kernels, kernels(): pl.pallas_call(functools.partial(exchange, fs_count, rep_count, tp_count)...  31.6 us
    pallas_call x1, Pallas kernels, kernels(): pl.pallas_call(finish, out_shape=tuple((jax.ShapeDtypeStruct(*x) for x in...  2.12 us

profile of v2, /device:TPU:0, one launch (start us, length us, event | category | flops | bytes accessed | tf_op | source)
XLA Modules:
  0.0 34.4 jit_solution(14151224139788845896)
XLA Ops:
  0.6 31.6 %exchange.1 = (f32[512,256]{1,0:T(8,128)S(1)}, f32[256,512]{1,0:T(8,128)S(1)}, f32[512,256]{1,0:T(8,128)S(1)}, f32[256,512]{1,0:T(8,128)S(1)}, bf16[2048,256]{1,...) custom-call(bf16[896,2048]{1,0:T(8,128)(2,1)} %hidden.1, ...), custom_call_target="tpu_custom_call" | custom-call | tf_op jit(solution)/shard_map/exchange/pallas_call | solution.py:575
  32.2 2.1 %finish.1 = (f32[512,256]{1,0:T(8,128)}, f32[256,512]{1,0:T(8,128)}, f32[512,256]{1,0:T(8,128)}, f32[256,512]{1,0:T(8,128)}, bf16[2048,256]{1,0:T(8,128)(2,1)}, ...) custom-call(f32[512,256]{1,0:T(8,128)S(1)} %get-tuple-element.20.ref, ...), custom_call_target="tpu_custom_call" | custom-call | tf_op jit(solution)/shard_map/finish/pallas_call | solution.py:609

commit v3 on v2

--- a/solution.py
+++ b/solution.py
@@ -13,9 +13,12 @@
 PIECES = 2
 EXTRA = 1
 EARLY = 4
-AHEAD = 4
-LATE = 4
+AHEAD = 2
+SOON = 1
+LAST = 2
+PEEK_AT = (6,)
 VMEM_LIMIT = 59 * 1024 * 1024
+FINISH_LIMIT = 16 * 1024 * 1024
 MEETINGS = 3
 MEET_AT = (1, 3, 5)
 
@@ -126,43 +129,18 @@
     fs_count, rep_count, tp_count,
     hidden, grad_value, mixed, grad_output, basis_value, basis_output, weight_value, weight_output,
     first_value, second_value, first_output, second_output,
-    *refs,
+    direction, owned, clip, all_value, all_output, value_in, output_in, basis_in, moment_in,
+    tokens_in, thin_in, part, part_sent, landed, halves, squares_all,
+    load_sem, sent_sem, near_recv, side_recv, part_recv, half_recv, square_recv, turn_recv, ready,
 ):
-    targets, made, refs = refs[:10], refs[10:20], refs[20:]
-    (
-    tokens_in, thin_in, basis_in, value_in, output_in, moment_in, all_value, all_output,
-    part, part_sent, landed, squares_all, owned, direction,
-    load_sem, sent_sem, near_recv, side_recv, part_recv, square_recv, owned_recv, turn_recv,
-    ready, store_sem,
-    ) = refs
-    step_value, step_output, new_value, new_output, copy_value, copy_output = made[:6]
-    group = fs_count * rep_count
-    everyone = group * tp_count
+    ring = fs_count * tp_count
     fs, rep, tp = lax.axis_index("fs"), lax.axis_index("rep"), lax.axis_index("tp")
-    me = fs * rep_count + rep
-    at_end = jnp.logical_or(fs == 0, fs == fs_count - 1)
+    other_rep = lax.rem(rep + 1, rep_count)
     tokens = hidden.shape[0]
     count, width = value_in.shape
     rows = part.shape[2]
     piece = tokens // TOKEN_PIECES
     f32, bf16 = jnp.float32, jnp.bfloat16
-
-    stores = []
-
-    def store(i, here=None, there=None):
-        def make():
-            source, target = made[i], targets[i]
-            if here is not None:
-                source, target = source.at[here], target.at[here]
-            return pltpu.make_async_copy(source, target, store_sem)
-
-        if there is None:
-            make().start()
-        else:
-            @pl.when(there)
-            def _():
-                make().start()
-        stores.append((there, make))
 
     loads = []
 
@@ -188,14 +166,8 @@
         for i, source in enumerate((first_value, first_output, second_value, second_output))
     ]
 
-    def member(k):
-        other = lax.rem(me + k, group)
-        return {"fs": other // rep_count, "rep": lax.rem(other, rep_count)}
-
-    def anyone(k):
-        other = lax.rem(me * tp_count + tp + k, everyone)
-        at = other // tp_count
-        return {"fs": at // rep_count, "rep": lax.rem(at, rep_count), "tp": lax.rem(other, tp_count)}
+    def along(k):
+        return lax.rem(fs + k, fs_count)
 
     def signal(sem, **where):
         pl.semaphore_signal(sem, inc=1, device_id=where, device_id_type=MESH)
@@ -218,8 +190,6 @@
 
     pl.semaphore_wait(barrier, beside + (rep_count - 1 + tp_count - 1))
     signal_beside(ready.at[0])
-    for j in range(1, rep_count):
-        signal(ready.at[0], rep=lax.rem(rep + j, rep_count))
     inputs, buffers = (value_in, output_in), (all_value, all_output)
 
     def cast(owner_rep):
@@ -233,7 +203,7 @@
     cast(rep)
 
     def meet(k):
-        pl.semaphore_wait(ready.at[k], beside + (rep_count - 1 if k == 0 else 0))
+        pl.semaphore_wait(ready.at[k], beside)
         if k + 1 < MEETINGS:
             signal_beside(ready.at[k + 1])
 
@@ -359,13 +329,12 @@
         return copy
 
     def send_part(a, total):
-        part[a] = total.reshape(group, rows, width)
-        part_sent[a] = total.astype(bf16).reshape(group, rows, width)
-        for k in range(1, group):
-            other = lax.rem(me + k, group)
+        part[a] = total.reshape(fs_count, rows, width)
+        part_sent[a] = total.astype(bf16).reshape(fs_count, rows, width)
+        for k in range(1, fs_count):
             send(remote(
-                part_sent.at[a, other], landed.at[a, k - 1],
-                sent_sem, part_recv.at[a], **member(k),
+                part_sent.at[a, along(k)], landed.at[a, k - 1], sent_sem, part_recv.at[a],
+                fs=along(k),
             ))
 
     send_own(own_items[:EARLY])
@@ -378,7 +347,7 @@
         product = split_product(reduced, thin_in[a, pl.ds(c * piece, piece)])
         totals[a] = product if totals[a] is None else totals[a] + product
 
-    met = 0
+    met = peeked = 0
     for a in range(2):
         first, blocks = stream_loads[a]
         for copy in first:
@@ -391,140 +360,81 @@
             if pending is not None:
                 finish_piece(*pending)
             pending = (a, c, reduced)
+            if a * TOKEN_PIECES + c in PEEK_AT:
+                pass_on(1, own_items[peeked : peeked + 1])
+                peeked += 1
             if a * TOKEN_PIECES + c in MEET_AT:
                 meet(met)
                 met += 1
                 if met == MEETINGS:
                     send_part(0, totals[0])
-                    send_own(own_items[EARLY:])
     finish_piece(*pending)
+    if met < MEETINGS:
+        meet(met)
+        send_part(0, totals[0])
     send_part(1, totals[1])
+    send_own(own_items[EARLY:])
     send_own(far_items + rest_items)
-    pass_on(1, own_items)
+    pass_on(1, own_items[peeked:])
     for a in range(2):
         arrived(landed.at[a], part_recv.at[a])
-    squares = jnp.zeros((rows, width), f32)
-    for a in range(2):
-        summed = part[a, me]
-        for k in range(group - 1):
+        summed = part[a, fs]
+        for k in range(fs_count - 1):
             summed = summed + landed[a, k].astype(f32)
-        owned[rep, a] = summed
-        squares = squares + summed * summed
-    place = me * tp_count + tp
-    squares_all[place] = jnp.full(squares_all.shape[1:], jnp.sum(squares), f32)
-    for k in range(1, everyone):
-        send(remote(
-            squares_all.at[place], squares_all.at[place],
-            sent_sem, square_recv, **anyone(k),
-        ))
-    owned_copies = [
-        send(remote(
-            owned.at[rep], owned.at[rep], sent_sem, owned_recv.at[j - 1],
-            rep=lax.rem(rep + j, rep_count),
-        ))
-        for j in range(1, rep_count)
-    ]
+        halves[rep, a] = summed.astype(bf16)
+        mine = halves.at[rep, a]
+        send(remote(mine, mine, sent_sem, half_recv.at[a], rep=other_rep))
     pass_on(1, far_items)
     for d in range(2, fs_count - 1):
         pass_on(d, own_items[:AHEAD])
-        pass_on(d, own_items[AHEAD:], at_end)
+    squares = jnp.zeros((rows, width), f32)
+    for a in range(2):
+        arrived(halves.at[other_rep, a], half_recv.at[a])
+        summed = halves[0, a].astype(f32)
+        for r in range(1, rep_count):
+            summed = summed + halves[r, a].astype(f32)
+        owned[a] = summed
+        squares = squares + summed * summed
+    place = fs * tp_count + tp
+    squares_all[place] = jnp.full(squares_all.shape[1:], jnp.sum(squares), f32)
+    for k in range(1, ring):
+        other = lax.rem(place + k, ring)
+        send(remote(
+            squares_all.at[place], squares_all.at[place], sent_sem, square_recv,
+            fs=other // tp_count, tp=lax.rem(other, tp_count),
+        ))
+    for d in range(2, fs_count - 1):
+        pass_on(d, own_items[AHEAD:])
+        pass_on(d, far_items[:SOON])
+    pass_on(fs_count - 1, own_items[:LAST])
     for copy in moment_loads:
         copy.wait()
-    arrived(squares_all.at[pl.ds(0, everyone - 1)], square_recv)
+    arrived(squares_all.at[pl.ds(0, ring - 1)], square_recv)
     mean_square = jnp.sum(squares_all[...], axis=0) / (2 * RANK * AW)
     factor = jnp.minimum(1.0, 1.0 / jnp.sqrt(mean_square + norm_epsilon))
+    clip[...] = jnp.broadcast_to(factor, clip.shape)
     scale = factor[:1, :1]
-    mine_rows = pl.ds(pl.multiple_of(rep * rows, rows), rows)
     for a in range(2):
-        _, _, turned = moments(
-            owned[rep, a], moment_in[a, mine_rows], moment_in[2 + a, mine_rows], scale
-        )
-        direction[me, a] = turned.astype(bf16)
-    for k in range(1, group):
-        send(remote(
-            direction.at[me], direction.at[me], sent_sem, turn_recv, **member(k)
-        ))
+        _, _, turned = moments(owned[a], moment_in[a], moment_in[2 + a], scale)
+        direction[fs, a] = turned.astype(bf16)
+    for k in range(1, fs_count):
+        send(remote(direction.at[fs], direction.at[fs], sent_sem, turn_recv, fs=along(k)))
     for d in range(2, fs_count - 1):
-        pass_on(d, own_items[AHEAD:], jnp.logical_not(at_end))
-        pass_on(d, far_items)
-    pass_on(fs_count - 1, own_items[:LATE])
-    arrived(direction.at[pl.ds(0, group - 1)], turn_recv)
-
-    over = (((1,), (1,)), ((), ()))
-    turn_value = direction[:, 0].reshape(RANK, width)
-    turn_output = direction[:, 1].reshape(RANK, width).astype(f32).T.astype(bf16)
-
-    def here(f):
-        return pl.ds(pl.multiple_of(f * count, count), count)
-
-    def value_step(f):
-        return jnp.dot(basis_in[0, here(f)], turn_value, preferred_element_type=f32)
-
-    def output_step(f):
-        return lax.dot_general(turn_output, basis_in[1, here(f)], over, preferred_element_type=f32)
-
-    def move(weight, step):
-        return (weight.astype(f32) - learning_rate * step).astype(bf16)
-
-    step = value_step(fs)
-    step_value[...] = step
-    store(0)
-    new_value[...] = value_in[...] - learning_rate * step
-    store(2)
-    copy_value[here(fs)] = move(all_value[fs], step)
-    store(4, here(fs))
-    step = output_step(fs)
-    step_output[...] = step
-    store(1)
-    new_output[...] = output_in[...] - learning_rate * step
-    store(3)
-    copy_output[:, here(fs)] = move(all_output[fs], step)
-    store(5, (slice(None), here(fs)))
-
-    def settle(d, a):
-        for way in range(2):
-            if d == 1:
-                for item in rest_items:
-                    if item[1] == a:
-                        @pl.when(comes(way, d, item))
-                        def _():
-                            arrival(way, d, item).wait_recv()
+        pass_on(d, far_items[SOON:])
+    pass_on(fs_count - 1, own_items[LAST:] + far_items)
+    for way in range(2):
+        for item in rest_items:
+            @pl.when(comes(way, 1, item))
+            def _():
+                arrival(way, 1, item).wait_recv()
+        for d in range(1, fs_count):
             for item in own_items:
-                if item[1] == a:
-                    there = crosses(way, d, item)
-                    if there is not None:
-                        @pl.when(there)
-                        def _():
-                            across(way, d, item, 1).wait_recv()
-
-            f = fs - step_of(way) * d
-            at = here(f)
-            held_there = reaches(way, d)
-
-            @pl.when(held_there)
-            def _():
-                if a == 0:
-                    copy_value[at] = move(all_value[f], value_step(f))
-                else:
-                    copy_output[:, at] = move(all_output[f], output_step(f))
-
-            store(4 + a, at if a == 0 else (slice(None), at), held_there)
-
-    for a in range(2):
-        settle(1, a)
-    pass_on(fs_count - 1, own_items[LATE:] + far_items)
-
-    for copy in owned_copies:
-        copy.wait_recv()
-    for a in range(2):
-        made[6 + 2 * a][...], made[7 + 2 * a][...], _ = moments(
-            owned[:, a].reshape(moment_in.shape[1:]), moment_in[a], moment_in[2 + a], scale
-        )
-        store(6 + 2 * a)
-        store(7 + 2 * a)
-    for d in range(2, fs_count):
-        for a in range(2):
-            settle(d, a)
+                there = crosses(way, d, item)
+                if there is not None:
+                    @pl.when(there)
+                    def _():
+                        across(way, d, item, 1).wait_recv()
+    arrived(direction.at[pl.ds(0, fs_count - 1)], turn_recv)
 
     for copy in sent:
         copy.wait_send()
@@ -533,24 +443,65 @@
         def _():
             make().wait_send()
 
-    for there, make in stores:
-        if there is None:
-            make().wait()
-        else:
-            @pl.when(there)
-            def _():
-                make().wait()
-
-
-def finish(*refs):
-    made = len(refs) // 2
-    sources, targets, sem = refs[:made], refs[made : 2 * made], refs[-1]
-    copies = [
-        pltpu.make_async_copy(sources[i], targets[i], sem.at[i]) for i in range(made)
-    ]
-    for copy in copies:
+
+def finish(
+    direction, owned, clip, all_value, all_output, value_in, output_in, basis_in, moment_in, *refs
+):
+    count = len(refs) // 2
+    targets, made, sem = refs[:count], refs[count : 2 * count], refs[-1]
+    f32, bf16 = jnp.float32, jnp.bfloat16
+    fs_count, rows_each, width = all_value.shape
+    fs = lax.axis_index("fs")
+    over = (((1,), (1,)), ((), ()))
+    stores = []
+
+    def store(i, here=None):
+        source, target = made[i], targets[i]
+        if here is not None:
+            source, target = source.at[here], target.at[here]
+        copy = pltpu.make_async_copy(source, target, sem)
         copy.start()
-    for copy in copies:
+        stores.append(copy)
+
+    turn_value = direction[:, 0].reshape(RANK, width)
+    turn_output = direction[:, 1].reshape(RANK, width).astype(f32).T.astype(bf16)
+
+    def value_step(here):
+        return jnp.dot(basis_in[0, here], turn_value, preferred_element_type=f32)
+
+    def output_step(here):
+        return lax.dot_general(turn_output, basis_in[1, here], over, preferred_element_type=f32)
+
+    def move(weight, step):
+        return (weight.astype(f32) - learning_rate * step).astype(bf16)
+
+    mine = pl.ds(pl.multiple_of(fs * rows_each, rows_each), rows_each)
+    step = value_step(mine)
+    made[0][...] = step
+    store(0)
+    made[2][...] = value_in[...] - learning_rate * step
+    store(2)
+    step = output_step(mine)
+    made[1][...] = step
+    store(1)
+    made[3][...] = output_in[...] - learning_rate * step
+    store(3)
+    for f in range(fs_count):
+        here = pl.ds(f * rows_each, rows_each)
+        made[4][here] = move(all_value[f], value_step(here))
+        store(4, here)
+    for f in range(fs_count):
+        here = pl.ds(f * rows_each, rows_each)
+        made[5][:, here] = move(all_output[f], output_step(here))
+        store(5, (slice(None), here))
+    scale = clip[:1, :1]
+    for a in range(2):
+        made[6 + 2 * a][...], made[7 + 2 * a][...], _ = moments(
+            owned[a], moment_in[a], moment_in[2 + a], scale
+        )
+        store(6 + 2 * a)
+        store(7 + 2 * a)
+    for copy in stores:
         copy.wait()
 
 
@@ -559,44 +510,42 @@
     saved_hidden, grad_value, saved_mixed, grad_output, basis_value, basis_output,
     weight_value, weight_output, first_value, second_value, first_output, second_output,
 ):
-    group = fs_count * rep_count
     tokens, model = saved_hidden.shape
     count, width = weight_value.shape
     rank = basis_value.shape[1]
-    rows = rank // group
+    rows = rank // fs_count
     f32, bf16 = jnp.float32, jnp.bfloat16
     dma = pltpu.SemaphoreType.DMA
     anywhere = pl.BlockSpec(memory_space=pl.ANY)
+    in_vmem = pl.BlockSpec(memory_space=pltpu.VMEM)
     moment = (first_value.shape, f32)
     results = (
         ((count, width), f32), ((width, count), f32), ((count, width), f32), ((width, count), f32),
         ((model, width), bf16), ((width, model), bf16), moment, moment, moment, moment,
     )
-    made = pl.pallas_call(
+    kept = (
+        ((fs_count, 2, rows, width), bf16), ((2, rows, width), f32), ((8, 128), f32),
+        ((fs_count, count, width), bf16), ((fs_count, width, count), bf16),
+        ((count, width), f32), ((width, count), f32),
+        ((2, model, rank), bf16), ((4,) + first_value.shape, f32),
+    )
+    held = pl.pallas_call(
         functools.partial(exchange, fs_count, rep_count, tp_count),
-        out_shape=tuple(pltpu.VMEM(*x) for x in results),
+        out_shape=tuple(pltpu.VMEM(*x) for x in kept),
         in_specs=[anywhere] * 12,
-        out_specs=(anywhere,) * len(results),
-        scratch_shapes=[pltpu.VMEM(*x) for x in results]
-        + [
+        out_specs=(in_vmem,) * len(kept),
+        scratch_shapes=[
             pltpu.VMEM((2, tokens, model), bf16),
             pltpu.VMEM((2, tokens, width), bf16),
-            pltpu.VMEM((2, model, rank), bf16),
-            pltpu.VMEM((count, width), f32),
-            pltpu.VMEM((width, count), f32),
-            pltpu.VMEM((4,) + first_value.shape, f32),
-            pltpu.VMEM((fs_count, count, width), bf16),
-            pltpu.VMEM((fs_count, width, count), bf16),
-            pltpu.VMEM((2, group, rows, width), f32),
-            pltpu.VMEM((2, group, rows, width), bf16),
-            pltpu.VMEM((2, group - 1, rows, width), bf16),
-            pltpu.VMEM((group * tp_count, 1, 128), f32),
-            pltpu.VMEM((rep_count, 2, rows, width), f32),
-            pltpu.VMEM((group, 2, rows, width), bf16),
+            pltpu.VMEM((2, fs_count, rows, width), f32),
+            pltpu.VMEM((2, fs_count, rows, width), bf16),
+            pltpu.VMEM((2, fs_count - 1, rows, width), bf16),
+            pltpu.VMEM((rep_count, 2, rows, width), bf16),
+            pltpu.VMEM((fs_count * tp_count, 1, 128), f32),
             dma((10 + 2 * TOKEN_PIECES,)), dma,
             dma((fs_count - 1, rep_count, 2, PIECES)), dma((fs_count - 1, 2, PIECES)),
-            dma((2,)), dma, dma((rep_count - 1,)), dma,
-            pltpu.SemaphoreType.REGULAR((MEETINGS,)), dma,
+            dma((2,)), dma((2,)), dma, dma,
+            pltpu.SemaphoreType.REGULAR((MEETINGS,)),
         ],
         compiler_params=pltpu.CompilerParams(
             collective_id=0, has_side_effects=True, vmem_limit_bytes=VMEM_LIMIT
@@ -609,12 +558,12 @@
     return pl.pallas_call(
         finish,
         out_shape=tuple(jax.ShapeDtypeStruct(*x) for x in results),
-        in_specs=[anywhere] * len(results),
+        in_specs=[in_vmem] * len(kept),
         out_specs=(anywhere,) * len(results),
-        scratch_shapes=[dma((len(results),))],
-        compiler_params=pltpu.CompilerParams(vmem_limit_bytes=1024 * 1024),
+        scratch_shapes=[pltpu.VMEM(*x) for x in results] + [dma],
+        compiler_params=pltpu.CompilerParams(vmem_limit_bytes=FINISH_LIMIT),
         name="finish",
-    )(*made)
+    )(*held)
 
 
 def solution(mesh):

time: 34.5 us -> 32.9 us (0.954)
  Pallas kernels: 33.7 us -> 32 us
    pallas_call x1, Pallas kernels: 31.6 us -> 29.7 us  [kernels(): pl.pallas_call(functools.partial(exchange, fs_count, rep_count, tp_count)...]
where the time goes in v3:
time: 32.9 us; the launch traced here: 32.7 us
  Pallas kernels  32 us (97%)
  between operations  0.66 us (2%)
    pallas_call x1, Pallas kernels, kernels(): pl.pallas_call(functools.partial(exchange, fs_count, rep_count, tp_count)...  29.7 us
    pallas_call x1, Pallas kernels, kernels(): pl.pallas_call(finish, out_shape=tuple((jax.ShapeDtypeStruct(*x) for x in...  2.32 us

profile of v3, /device:TPU:0, one launch (start us, length us, event | category | flops | bytes accessed | tf_op | source)
XLA Modules:
  0.0 32.7 jit_solution(3484887848149308685)
XLA Ops:
  0.6 29.7 %exchange.1 = (bf16[4,2,32,256]{3,2,1,0:T(8,128)(2,1)S(1)}, f32[2,32,256]{2,1,0:T(8,128)S(1)}, f32[8,128]{1,0:T(8,128)S(1)}, bf16[4,512,256]{2,1,0:T(8,128)(2,1)...) custom-call(bf16[896,2048]{1,0:T(8,128)(2,1)} %hidden.1, ...), custom_call_target="tpu_custom_call" | custom-call | tf_op jit(solution)/shard_map/exchange/pallas_call | solution.py:532
  30.4 2.3 %finish.1 = (f32[512,256]{1,0:T(8,128)}, f32[256,512]{1,0:T(8,128)}, f32[512,256]{1,0:T(8,128)}, f32[256,512]{1,0:T(8,128)}, bf16[2048,256]{1,0:T(8,128)(2,1)}, ...) custom-call(bf16[4,2,32,256]{3,2,1,0:T(8,128)(2,1)S(1)} %get-tuple-e, ...), custom_call_target="tpu_custom_call" | custom-call | tf_op jit(solution)/shard_map/finish/pallas_call | solution.py:558

commit v4 on v3

--- a/solution.py
+++ b/solution.py
@@ -20,7 +20,8 @@
 VMEM_LIMIT = 59 * 1024 * 1024
 FINISH_LIMIT = 16 * 1024 * 1024
 MEETINGS = 3
-MEET_AT = (1, 3, 5)
+MEET_AT = (1, 3)
+MIDDLE = 4
 
 
 first_decay = 0.8
@@ -215,7 +216,7 @@
         return buffers[a].at[f, pl.ds(start, spans[a])]
 
     own_items = [(0, a, q) for a in range(2) for q in range(PIECES)]
-    far_items = [(1, 1, q) for q in range(EXTRA)]
+    far_items = [(1, 1, PIECES - 1 - q) for q in range(EXTRA)]
     rest_items = [(1, a, q) for a in range(2) for q in range(PIECES) if (1, a, q) not in far_items]
 
     def both(x, y):
@@ -359,6 +360,9 @@
             )
             if pending is not None:
                 finish_piece(*pending)
+                if pending[1] == TOKEN_PIECES - 1:
+                    send_part(0, totals[0])
+                    send_own(own_items[EARLY:MIDDLE])
             pending = (a, c, reduced)
             if a * TOKEN_PIECES + c in PEEK_AT:
                 pass_on(1, own_items[peeked : peeked + 1])
@@ -366,14 +370,9 @@
             if a * TOKEN_PIECES + c in MEET_AT:
                 meet(met)
                 met += 1
-                if met == MEETINGS:
-                    send_part(0, totals[0])
     finish_piece(*pending)
-    if met < MEETINGS:
-        meet(met)
-        send_part(0, totals[0])
     send_part(1, totals[1])
-    send_own(own_items[EARLY:])
+    send_own(own_items[MIDDLE:])
     send_own(far_items + rest_items)
     pass_on(1, own_items[peeked:])
     for a in range(2):
@@ -387,6 +386,7 @@
     pass_on(1, far_items)
     for d in range(2, fs_count - 1):
         pass_on(d, own_items[:AHEAD])
+    meet(met)
     squares = jnp.zeros((rows, width), f32)
     for a in range(2):
         arrived(halves.at[other_rep, a], half_recv.at[a])

time: 32.9 us -> 32.6 us (level)
  no operation moved by 1% of the time
where the time goes in v4:
time: 32.6 us; the launch traced here: 32.4 us
  Pallas kernels  31.8 us (98%)
  between operations  0.66 us (2%)
    pallas_call x1, Pallas kernels, kernels(): pl.pallas_call(functools.partial(exchange, fs_count, rep_count, tp_count)...  29.4 us
    pallas_call x1, Pallas kernels, kernels(): pl.pallas_call(finish, out_shape=tuple((jax.ShapeDtypeStruct(*x) for x in...  2.32 us

profile of v4, /device:TPU:0, one launch (start us, length us, event | category | flops | bytes accessed | tf_op | source)
XLA Modules:
  0.0 32.4 jit_solution(6678816601056122404)
XLA Ops:
  0.6 29.4 %exchange.1 = (bf16[4,2,32,256]{3,2,1,0:T(8,128)(2,1)S(1)}, f32[2,32,256]{2,1,0:T(8,128)S(1)}, f32[8,128]{1,0:T(8,128)S(1)}, bf16[4,512,256]{2,1,0:T(8,128)(2,1)...) custom-call(bf16[896,2048]{1,0:T(8,128)(2,1)} %hidden.1, ...), custom_call_target="tpu_custom_call" | custom-call | tf_op jit(solution)/shard_map/exchange/pallas_call | solution.py:532
  30.1 2.3 %finish.1 = (f32[512,256]{1,0:T(8,128)}, f32[256,512]{1,0:T(8,128)}, f32[512,256]{1,0:T(8,128)}, f32[256,512]{1,0:T(8,128)}, bf16[2048,256]{1,0:T(8,128)(2,1)}, ...) custom-call(bf16[4,2,32,256]{3,2,1,0:T(8,128)(2,1)S(1)} %get-tuple-e, ...), custom_call_target="tpu_custom_call" | custom-call | tf_op jit(solution)/shard_map/finish/pallas_call | solution.py:558
